TPU v7x, 32 devices: a whole 2x2x4 slice. The times are simulated.
32 devices in a mesh: fs: 8 (over z, x), tp: 4 (over y, core).
Axes of the slice: x: 2, y: 2, z: 4, core: 2. Of those that a mesh axis runs over, the one named last changes fastest.
Arguments:
- normed_input: bfloat16 [16384, 2048], P('fs'), may hold values from -6 to 6
- forget_cot: bfloat16 [16384, 2048], P('fs', 'tp'), may hold values from -6 to 6
- value_cot: bfloat16 [16384, 2048], P('fs', 'tp'), may hold values from -6 to 6
- gated_output: bfloat16 [16384, 2048], P('fs', 'tp'), may hold values from -6 to 6
- output_cot: bfloat16 [16384, 2048], P('fs'), may hold values from -6 to 6
- forget_weight: float32 [2048, 2048], P('fs', 'tp'), may hold values from -0.125 to 0.125
- value_weight: float32 [2048, 2048], P('fs', 'tp'), may hold values from -0.125 to 0.125
- out_weight: float32 [2048, 2048], P('tp', 'fs'), may hold values from -0.125 to 0.125
- bases: bfloat16 [3, 2048, 256], replicated, may hold values from -0.125 to 0.125
- first_moment: float32 [256, 3, 2048], P('fs', None, 'tp'), may hold values from -4 to 4
- second_moment: float32 [256, 3, 2048], P('fs', None, 'tp'), may hold values from 0.25 to 4
Outputs:
- new_forget: float32 [2048, 2048], P('fs', 'tp')
- new_value: float32 [2048, 2048], P('fs', 'tp')
- new_out: float32 [2048, 2048], P('tp', 'fs')
- copy_forget: bfloat16 [2048, 2048], P(None, 'tp')
- copy_value: bfloat16 [2048, 2048], P(None, 'tp')
- copy_out: bfloat16 [2048, 2048], P('tp')
- moment_one: float32 [256, 3, 2048], P('fs', None, 'tp')
- moment_two: float32 [256, 3, 2048], P('fs', None, 'tp')
- step_forget: float32 [2048, 2048], P('fs', 'tp')
- step_value: float32 [2048, 2048], P('fs', 'tp')
- step_out: float32 [2048, 2048], P('tp', 'fs')
All inputs are finite; a program needn't handle non-finite values.
Results may differ from a plain program's by a relative error of at most 0.0045.
Values may be sent and summed in bfloat16 or wider, within the bound.
A program may use at most 128 MiB of HBM per device.

v0:
```python
import jax
import jax.numpy as jnp
from jax import lax
from jax.sharding import PartitionSpec as P


def split_parts(values):
    high = lax.optimization_barrier(values.astype(jnp.bfloat16))
    low = (values - high.astype(jnp.float32)).astype(jnp.bfloat16)
    return (high, low)


def on_device(
    normed_input,
    forget_cot,
    value_cot,
    gated_output,
    output_cot,
    forget_weight,
    value_weight,
    out_weight,
    bases,
    first_moment,
    second_moment,
):
    rows = forget_weight.shape[0]
    rank_rows = first_moment.shape[0]
    columns = forget_weight.shape[1]
    offset = lax.axis_index("fs") * rows
    factor = float(normed_input.shape[0] * lax.axis_size("fs")) ** (-0.5)
    my_bases = lax.dynamic_slice_in_dim(bases, offset, rows, 1)
    reduced = jnp.stack(
        [
            jnp.dot(normed_input, bases[0], preferred_element_type=jnp.float32),
            jnp.dot(normed_input, bases[1], preferred_element_type=jnp.float32),
            jnp.dot(output_cot, bases[2], preferred_element_type=jnp.float32),
        ],
        axis=1,
    )
    reduced_high, reduced_low = split_parts(reduced)
    paired = jnp.stack([forget_cot, value_cot, gated_output], axis=1)
    upper = jnp.einsum("tkr,tkc->rkc", reduced_high, paired, preferred_element_type=jnp.float32)
    lower = jnp.einsum("tkr,tkc->rkc", reduced_low, paired, preferred_element_type=jnp.float32)
    projected = lax.psum_scatter(
        ((upper + lower) * factor).astype(jnp.bfloat16), "fs", scatter_dimension=0, tiled=True
    ).astype(jnp.float32)
    moment_one = 0.9 * first_moment + 0.1 * projected
    moment_two = 0.9 * second_moment + 0.1 * projected * projected
    direction = moment_one / (jnp.sqrt(moment_two) + 1e-08)
    piece_high, piece_low = split_parts(lax.all_gather(direction, "fs", axis=0, tiled=True))
    upper = jnp.einsum("kdr,rkc->dkc", my_bases, piece_high, preferred_element_type=jnp.float32)
    lower = jnp.einsum("kdr,rkc->dkc", my_bases, piece_low, preferred_element_type=jnp.float32)
    full = upper + lower
    totals = lax.psum(jnp.sum(direction * direction, axis=(0, 2)), ("fs", "tp"))
    entries = rank_rows * lax.axis_size("fs") * columns * lax.axis_size("tp")
    scale = lax.rsqrt(totals / entries + 1.0)
    full = full * scale[None, :, None]
    step_forget = full[:, 0, :]
    step_value = full[:, 1, :]
    step_out = full[:, 2, :].T
    new_forget = forget_weight - 0.01 * step_forget
    new_value = value_weight - 0.01 * step_value
    new_out = out_weight - 0.01 * step_out
    copy_forget, copy_value, copy_out = (
        lax.all_gather(new_forget.astype(jnp.bfloat16), "fs", axis=0, tiled=True),
        lax.all_gather(new_value.astype(jnp.bfloat16), "fs", axis=0, tiled=True),
        lax.all_gather(new_out.astype(jnp.bfloat16), "fs", axis=1, tiled=True),
    )
    return (
        new_forget,
        new_value,
        new_out,
        copy_forget,
        copy_value,
        copy_out,
        moment_one,
        moment_two,
        step_forget,
        step_value,
        step_out,
    )


def solution(mesh):
    placed = (
        P("fs", None),
        P("fs", "tp"),
        P("fs", "tp"),
        P("fs", "tp"),
        P("fs", None),
        P("fs", "tp"),
        P("fs", "tp"),
        P("tp", "fs"),
        P(),
        P("fs", None, "tp"),
        P("fs", None, "tp"),
    )
    return jax.shard_map(
        on_device,
        mesh=mesh,
        in_specs=placed,
        out_specs=(
            P("fs", "tp"),
            P("fs", "tp"),
            P("tp", "fs"),
            P(None, "tp"),
            P(None, "tp"),
            P("tp", None),
            P("fs", None, "tp"),
            P("fs", None, "tp"),
            P("fs", "tp"),
            P("fs", "tp"),
            P("tp", "fs"),
        ),
        check_vma=False,
    )
```

profile of v0, /device:TPU:0, one launch (start us, length us, event | category | flops | bytes accessed | tf_op | source)
XLA Modules:
  0.0 339.7 jit_solution(3506734847928019241)
XLA Ops:
  7.2 0.0 copy-start.13
  7.2 0.0 all-reduce.3.cloned.1.call-start
  7.2 0.0 copy-start.16
  7.2 0.0 slice-start
  7.3 6.2 %convolution_bitcast_fusion.1 = f32[2048,1,256]{2,0,1:T(8,128)S(1)} fusion(bf16[2048,2048]{1,0:T(8,128)(2,1)} %param.11, bf16[3,2048,256]{2,1,0:T(8,128)(2,1)} %param.19), kind=kOutput, calls=%fused_computation.6 | convolution fusion | flops 2147483648 | bytes 11534336 | tf_op jit(solution)/shard_map/dot_general | solution.py:35
  13.5 0.0 copy-done.13
  13.5 0.7 copy-done.16
  14.2 2.5 convolution_bitcast_fusion.2
  16.8 0.0 slice-done
  16.8 0.7 slice-done.1
  17.5 2.5 convolution_bitcast_fusion
  20.0 0.0 copy-done.5
  20.0 0.0 copy-done.7
  20.0 0.0 copy-start.9
  20.0 1.4 copy-done.9
  21.4 0.7 fusion
  22.0 3.9 %copy.56 = bf16[2048,512]{0,1:T(8,128)(2,1)} copy(bf16[2048,512]{1,0:T(8,128)(2,1)} %param.12) | data formatting | bytes 4194304 | tf_op args[1]
  25.9 3.9 %copy.57 = bf16[2048,512]{0,1:T(8,128)(2,1)} copy(bf16[2048,512]{1,0:T(8,128)(2,1)} %param.13) | data formatting | bytes 4194304 | tf_op args[2]
  29.8 3.9 %copy.58 = bf16[2048,512]{0,1:T(8,128)(2,1)} copy(bf16[2048,512]{1,0:T(8,128)(2,1)} %param.14) | data formatting | bytes 4194304 | tf_op args[3]
  33.8 0.0 copy-start.8
  33.8 0.0 copy-start.10
  33.8 4.6 %fusion.2 = f32[3,512,256]{2,1,0:T(8,128)S(1)} fusion(bf16[2048,3,256]{2,0,1:T(8,128)(2,1)S(1)} %fusion, bf16[2048,1,512]{0,2,1:T(8,128)(2,1)} %bitcast.47, bf16[2048,1,512]{0,2,1:T(8,128)(2,1)} %bitcast.45, bf16[2048,1,512]{0,2,1:T(8,128)(2,1)} %bitcast.43), kind=kOutput, calls=%fused_computation.8 | convolution fusion | flops 1616904192 | bytes 11010048 | tf_op jit(solution)/shard_map/tkr,tkc->rkc/dot_general | solution.py:42
  38.4 0.0 copy-done.2
  38.4 0.0 copy-done.3
  38.4 0.1 copy-done.4
  38.5 0.6 copy-done.6
  39.1 0.6 copy-done.8
  39.7 0.6 copy-done.10
  40.3 2.9 fusion.4
  43.2 2.7 copy.59
  45.9 0.0 all-reduce.3.cloned.1.call-update
  45.9 0.2 all-gather.5.cloned.1.call-start
  46.1 0.6 dynamic-slice
  47.4 79.8 %all-reduce.3.cloned.1.call-done = bf16[256,3,512]{2,1,0:T(4,128)(2,1)} async-done(((bf16[256,3,512]{2,1,0:T(4,128)(2,1)}), bf16[256,3,512]{2,1,0:T(4,128)(2,1)}) %all-reduce.3.cloned.1.call-update) | async-done | bytes 786448
  127.1 0.9 constant_dynamic-slice_fusion
  128.1 0.9 multiply_reduce_fusion
  129.1 0.0 all-gather.5.cloned.1.call-update
  129.1 0.0 all-gather.7.cloned.1.call-start
  129.1 0.2 copy.63
  129.4 1.0 copy.64
  130.4 40.3 %psum.7 = f32[3]{0:T(128)S(1)} all-reduce(f32[3]{0:T(128)S(1)} %get-tuple-element.51), channel_id=1, replica_groups=mesh['fs'=8,'tp'=4] {'fs','tp'}, use_global_device_ids=true, to_apply=%region_2.0 | all-reduce | flops 3 | bytes 24 | tf_op jit(solution)/shard_map/psum | solution.py:54
  170.7 3.3 all-gather.5.cloned.1.call-done
  174.0 1.6 convert_element_type.42
  175.6 1.5 fusion.12
  177.1 0.0 copy-start.1
  177.1 1.6 multiply_bitcast_fusion
  178.7 1.0 fusion.21
  179.6 0.0 all-gather.7.cloned.1.call-update
  179.7 0.0 all-gather.9.cloned.1.call-start
  179.7 0.5 all-gather.9.cloned.1.call-update
  180.2 0.0 all-gather.11.cloned.1.call-start
  180.3 2.2 fusion.20
  182.5 0.0 all-gather.11.cloned.1.call-update
  182.6 1.0 copy.65
  183.5 1.0 copy.66
  184.5 0.1 slice_bitcast_fusion.1
  184.6 1.0 copy.69
  185.6 1.0 copy.70
  186.6 42.0 %all-gather.7.cloned.1.call-done = bf16[2048,512]{0,1:T(8,128)(2,1)} async-done(((bf16[256,512]{0,1:T(8,128)(2,1)}), bf16[2048,512]{0,1:T(8,128)(2,1)}) %all-gather.7.cloned.1.call-update) | async-done | bytes 2097168 | tf_op jit(solution)/shard_map/all_gather | solution.py:65
  228.6 3.9 %copy.67 = bf16[2048,512]{1,0:T(8,128)(2,1)} copy(bf16[2048,512]{0,1:T(8,128)(2,1)} %all-gather.7.cloned.1.call-done) | data formatting | bytes 4194304
  232.5 47.1 %all-gather.9.cloned.1.call-done = bf16[2048,512]{0,1:T(8,128)(2,1)} async-done(((bf16[256,512]{0,1:T(8,128)(2,1)}), bf16[2048,512]{0,1:T(8,128)(2,1)}) %all-gather.9.cloned.1.call-update) | async-done | bytes 2097168 | tf_op jit(solution)/shard_map/all_gather | solution.py:66
  279.6 3.9 %copy.68 = bf16[2048,512]{1,0:T(8,128)(2,1)} copy(bf16[2048,512]{0,1:T(8,128)(2,1)} %all-gather.9.cloned.1.call-done) | data formatting | bytes 4194304
  283.5 46.5 %all-gather.11.cloned.1.call-done = bf16[512,2048]{1,0:T(8,128)(2,1)} async-done(((bf16[512,256]{1,0:T(8,128)(2,1)}), bf16[512,2048]{1,0:T(8,128)(2,1)}) %all-gather.11.cloned.1.call-update) | async-done | bytes 2097168 | tf_op jit(solution)/shard_map/all_gather | solution.py:67
  330.1 3.2 copy.79
  (22 shorter events, 0.0 us)
Async XLA Ops:
  7.2 6.3 %copy-start.13 = (bf16[3,2048,256]{2,1,0:T(8,128)(2,1)S(1)}, bf16[3,2048,256]{2,1,0:T(8,128)(2,1)}, u32[]{:S(2)}) copy-start(bf16[3,2048,256]{2,1,0:T(8,128)(2,1)} %param.19) | copy-start | bytes 9437188
  7.2 120.0 %all-reduce.3.cloned.1.call-start = ((), (), s32[]{:S(2)}) async-start(), calls=%async_computation.4 | async-start | bytes 2097152
  7.2 7.0 %copy-start.16 = (bf16[2048,2048]{1,0:T(8,128)(2,1)S(1)}, bf16[2048,2048]{1,0:T(8,128)(2,1)}, u32[]{:S(2)}) copy-start(bf16[2048,2048]{1,0:T(8,128)(2,1)} %param.11) | copy-start | bytes 25165828
  7.2 9.5 %slice-start = ((s8[8388608]{0:T(1024)(128)(4,1)}), s8[4194304]{0:T(1024)(128)(4,1)S(1)}, s32[]{:S(2)}) async-start(s8[8388608]{0:T(1024)(128)(4,1)} %bitcast.49), calls=%async_computation.5 | async-start | bytes 8388608
  14.2 5.8 %copy-start.5 = (f32[2048,1,256]{2,0,1:T(8,128)}, f32[2048,1,256]{2,0,1:T(8,128)S(1)}, u32[]{:S(2)}) copy-start(f32[2048,1,256]{2,0,1:T(8,128)S(1)} %convolution_bitcast_fusion.1) | copy-start | bytes 6291460
  14.2 3.3 slice-start.1
  17.5 2.5 copy-start.7
  20.0 1.4 copy-start.9
  33.8 4.6 %copy-start.2 = (bf16[2048,512]{0,1:T(8,128)(2,1)S(1)}, bf16[2048,512]{0,1:T(8,128)(2,1)}, u32[]{:S(2)}) copy-start(bf16[2048,512]{0,1:T(8,128)(2,1)} %copy.56) | copy-start | bytes 6291460
  33.8 4.6 %copy-start.3 = (bf16[2048,512]{0,1:T(8,128)(2,1)S(1)}, bf16[2048,512]{0,1:T(8,128)(2,1)}, u32[]{:S(2)}) copy-start(bf16[2048,512]{0,1:T(8,128)(2,1)} %copy.57) | copy-start | bytes 6291460
  33.8 4.7 %copy-start.4 = (bf16[2048,512]{0,1:T(8,128)(2,1)S(1)}, bf16[2048,512]{0,1:T(8,128)(2,1)}, u32[]{:S(2)}) copy-start(bf16[2048,512]{0,1:T(8,128)(2,1)} %copy.58) | copy-start | bytes 6291460
  33.8 5.3 %copy-start.6 = (f32[2048,1,256]{2,0,1:T(8,128)S(1)}, f32[2048,1,256]{2,0,1:T(8,128)}, u32[]{:S(2)}) copy-start(f32[2048,1,256]{2,0,1:T(8,128)} %copy-done.5) | copy-start | bytes 6291460
  33.8 5.9 %copy-start.8 = (f32[2048,1,256]{2,0,1:T(8,128)S(1)}, f32[2048,1,256]{2,0,1:T(8,128)}, u32[]{:S(2)}) copy-start(f32[2048,1,256]{2,0,1:T(8,128)} %copy-done.7) | copy-start | bytes 6291460
  33.8 6.5 %copy-start.10 = (f32[2048,1,256]{2,0,1:T(8,128)S(1)}, f32[2048,1,256]{2,0,1:T(8,128)}, u32[]{:S(2)}) copy-start(f32[2048,1,256]{2,0,1:T(8,128)} %copy-done.9) | copy-start | bytes 6291460
  43.2 2.9 copy-start.17
  43.2 84.9 %copy-start.14 = (f32[32,3,512]{2,0,1:T(8,128)S(1)}, f32[32,3,512]{2,0,1:T(8,128)}, u32[]{:S(2)}) copy-start(f32[32,3,512]{2,0,1:T(8,128)} %param.21) | copy-start | bytes 589828
  43.2 84.9 %copy-start.15 = (f32[32,3,512]{2,0,1:T(8,128)S(1)}, f32[32,3,512]{2,0,1:T(8,128)}, u32[]{:S(2)}) copy-start(f32[32,3,512]{2,0,1:T(8,128)} %param.20) | copy-start | bytes 589828
  43.2 86.0 %copy-start.11 = (f32[256,512]{1,0:T(8,128)S(1)}, f32[256,512]{1,0:T(8,128)}, u32[]{:S(2)}) copy-start(f32[256,512]{1,0:T(8,128)} %param.16) | copy-start | bytes 1572868
  45.9 83.5 %copy-start.12 = (f32[256,512]{1,0:T(8,128)S(1)}, f32[256,512]{1,0:T(8,128)}, u32[]{:S(2)}) copy-start(f32[256,512]{1,0:T(8,128)} %param.17) | copy-start | bytes 1572868
  45.9 128.1 %all-gather.5.cloned.1.call-start = ((), (), s32[]{:S(2)}) async-start(), calls=%async_computation | async-start | bytes 1769472 | tf_op jit(solution)/shard_map/all_gather | solution.py:50
  129.1 99.5 %all-gather.7.cloned.1.call-start = ((), (), s32[]{:S(2)}) async-start(), calls=%async_computation.1 | async-start | bytes 2359296 | tf_op jit(solution)/shard_map/all_gather | solution.py:65
  174.0 3.1 copy-start
  177.1 1.6 copy-start.1
  179.7 99.9 %all-gather.9.cloned.1.call-start = ((), (), s32[]{:S(2)}) async-start(), calls=%async_computation.2 | async-start | bytes 2359296 | tf_op jit(solution)/shard_map/all_gather | solution.py:66
  180.2 149.8 %all-gather.11.cloned.1.call-start = ((), (), s32[]{:S(2)}) async-start(), calls=%async_computation.3 | async-start | bytes 2359296 | tf_op jit(solution)/shard_map/all_gather | solution.py:67
Sparse Core Ops, SparseCore 0:
  46.0 81.0 all-reduce.2
  129.9 44.0 all-gather.4
  179.8 48.7 all-gather.6
  231.0 48.5 all-gather.8
  281.5 48.5 all-gather.10
where the time goes:
time: 340 us
  waiting for transfers between devices  219 us (64%)
  blocking collectives  40.3 us (12%)
  local copies, waits for them, and re-layouts  36.9 us (11%)
  matrix products  21.8 us (6%)
  between operations  14.7 us (4%)
  other arithmetic  6.41 us (2%)
    unnamed x6, waiting for transfers between devices  80.4 us
    all_gather x1, waiting for transfers between devices, on_device(): lax.all_gather(new_value.astype(jnp.bfloat16), 'fs', axis=0, tiled=True)  47.1 us
    all_gather x1, waiting for transfers between devices, on_device(): lax.all_gather(new_out.astype(jnp.bfloat16), 'fs', axis=1, tiled=True)  46.5 us
    all_gather x1, waiting for transfers between devices, on_device(): lax.all_gather(new_forget.astype(jnp.bfloat16), 'fs', axis=0, tiled=True)  42 us
    psum x1, blocking collectives, on_device(): totals = lax.psum(jnp.sum(direction * direction, axis=(0, 2)), ('fs', 'tp'))  40.3 us
    unnamed x54, local copies, waits for them, and re-layouts  34.2 us
  transfers between devices with their start and end apart: 5, of which 5 were waited for; matrix products, arithmetic and copies ran while one was open for 5% of the time, Pallas kernels for 0%

commit v1 on v0

v1 whole, which is shorter than its diff:
```python
import functools

import jax
import jax.numpy as jnp
from jax import lax
from jax.experimental import pallas as pl
from jax.experimental.pallas import tpu as pltpu
from jax.sharding import PartitionSpec as P

MESH = pl.DeviceIdType.MESH


def ring_index(place, size):
    back = lax.div(place, size // 2)
    return (1 - back) * 2 * place + back * (2 * (size - 1 - place) + 1)


def ring_place(index, size):
    odd = lax.rem(index, 2)
    half = lax.div(index, 2)
    return (1 - odd) * half + odd * (size - 1 - half)


def exchange_kernel(
    size,
    groups,
    factor,
    entries,
    x_hbm,
    oc_hbm,
    fc_hbm,
    vc_hbm,
    go_hbm,
    bases_hbm,
    fw_ref,
    vw_ref,
    ow_ref,
    m1_ref,
    m2_ref,
    all_f,
    all_v,
    all_o,
    dirs_out,
    scale_ref,
    n1_ref,
    n2_ref,
    x_buf,
    oc_buf,
    c_buf,
    b_buf,
    wf_buf,
    wv_buf,
    wo_buf,
    acc,
    part,
    got,
    mine,
    dirs,
    sums,
    load_sem,
    base_sem,
    put_sem,
    ring_send,
    ring_recv,
    part_send,
    part_recv,
    dir_send,
    dir_recv,
    sum_send,
    sum_recv,
):
    me = lax.axis_index("fs")
    mt = lax.axis_index("tp")
    place = ring_place(me, size)
    right = ring_index(lax.rem(place + 1, size), size)
    left = ring_index(lax.rem(place + size - 1, size), size)
    steps = size // 2
    tiles = load_sem.shape[1]
    tokens = x_buf.shape[0]
    rows_t = tokens // tiles
    rank_rows = m1_ref.shape[1]
    columns = m1_ref.shape[2]

    loads = []
    base_copies = [
        pltpu.make_async_copy(bases_hbm.at[k], b_buf.at[k], base_sem.at[k]) for k in range(3)
    ]

    def load(which, src, dst, tile):
        at = pl.ds(pl.multiple_of(tile * rows_t, rows_t), rows_t)
        return pltpu.make_async_copy(src.at[at, :], dst.at[at, :], load_sem.at[which, tile])

    streams = (
        (x_hbm, x_buf),
        (fc_hbm, c_buf.at[0]),
        (vc_hbm, c_buf.at[1]),
        (oc_hbm, oc_buf),
        (go_hbm, c_buf.at[2]),
    )
    base_copies[0].start()
    for tile in range(tiles):
        for which in (0, 1):
            load(which, *streams[which], tile).start()
    base_copies[1].start()
    for tile in range(tiles):
        load(2, *streams[2], tile).start()
    base_copies[2].start()
    for tile in range(tiles):
        for which in (3, 4):
            load(which, *streams[which], tile).start()

    barrier = pltpu.get_barrier_semaphore()
    for j in range(1, size):
        pl.semaphore_signal(
            barrier, inc=1, device_id=(lax.rem(me + j, size), mt), device_id_type=MESH
        )
    for j in range(1, groups):
        pl.semaphore_signal(
            barrier, inc=1, device_id=(me, lax.rem(mt + j, groups)), device_id_type=MESH
        )
    wf_buf[...] = fw_ref[...].astype(jnp.bfloat16)
    wv_buf[...] = vw_ref[...].astype(jnp.bfloat16)
    wo_buf[...] = ow_ref[...].astype(jnp.bfloat16)
    pl.semaphore_wait(barrier, size - 1 + groups - 1)

    def row_block(ref, owner, half):
        rows = wf_buf.shape[0]
        start, count = owner * rows, rows
        if half is not None:
            count = rows // 2
            start = start + half * count
        return ref.at[pl.ds(pl.multiple_of(start, count), count), :]

    def column_block(ref, owner, half):
        width = wo_buf.shape[1]
        lanes = pl.ds(pl.multiple_of(owner * width, width), width)
        height = wo_buf.shape[0]
        if half is None:
            return ref.at[:, lanes]
        return ref.at[pl.ds(half * (height // 2), height // 2), lanes]

    def dir_block(k, owner, half):
        at = pl.ds(pl.multiple_of(owner * rank_rows, rank_rows), rank_rows)
        if half is None:
            return dirs.at[k, at, :]
        return dirs.at[k, at, pl.ds(half * (columns // 2), columns // 2)]

    items = (
        (wf_buf, functools.partial(row_block, all_f)),
        (wv_buf, functools.partial(row_block, all_v)),
        (wo_buf, functools.partial(column_block, all_o)),
    )

    def hop(view, own, send_sem, recv_sem, item, step, way):
        sign = 1 if way == 0 else size - 1
        owner = ring_index(lax.rem(place + (size - sign) * (step - 1), size), size)
        half = way if step == steps else None
        dst = view(owner, half)
        src = own if own is not None and step == 1 and half is None else dst
        return pltpu.make_async_remote_copy(
            src_ref=src,
            dst_ref=dst,
            send_sem=send_sem.at[way, item, step - 1],
            recv_sem=recv_sem.at[way, item, step - 1],
            device_id=(right if way == 0 else left, mt),
            device_id_type=MESH,
        )

    def weight_hop(item, step, way):
        own, view = items[item]
        return hop(view, own, ring_send, ring_recv, item, step, way)

    def dir_hop(k, step, way):
        own = mine.at[k]
        return hop(functools.partial(dir_block, k), own, dir_send, dir_recv, k, step, way)

    puts = []
    for item in range(3):
        own, view = items[item]
        put = pltpu.make_async_copy(own, view(me, None), put_sem.at[item])
        put.start()
        puts.append(put)
        for way in range(2):
            weight_hop(item, 1, way).start()

    forwards = [(step, item) for step in range(2, steps + 1) for item in range(3)]

    def pump(count):
        for _ in range(min(count, len(forwards))):
            step, item = forwards.pop(0)
            for way in range(2):
                weight_hop(item, step - 1, way).wait_recv()
                weight_hop(item, step, way).start()

    def part_copy(k, j):
        owner = lax.rem(me + j, size)
        at = pl.ds(pl.multiple_of(owner * rank_rows, rank_rows), rank_rows)
        return pltpu.make_async_remote_copy(
            src_ref=part.at[k, at, :],
            dst_ref=got.at[k, j - 1],
            send_sem=part_send.at[k, j - 1],
            recv_sem=part_recv.at[k, j - 1],
            device_id=(owner, mt),
            device_id_type=MESH,
        )

    for k in range(3):
        base_copies[k].wait()
        left_which, right_which = ((0, 1), (0, 2), (3, 4))[k]
        source = x_buf if k < 2 else oc_buf
        acc[k] = jnp.zeros(acc.shape[1:], acc.dtype)

        def tile_body(tile, carry, k=k, left_which=left_which, right_which=right_which, source=source):
            at = pl.ds(pl.multiple_of(tile * rows_t, rows_t), rows_t)
            if k != 1:
                load(left_which, *streams[left_which], tile).wait()
            reduced = jnp.dot(
                source[at, :], b_buf[k], preferred_element_type=jnp.float32
            ).astype(jnp.bfloat16)
            load(right_which, *streams[right_which], tile).wait()
            acc[k] += lax.dot_general(
                reduced,
                c_buf[k, at, :],
                (((0,), (0,)), ((), ())),
                preferred_element_type=jnp.float32,
            )
            return carry

        lax.fori_loop(0, tiles, tile_body, 0)
        part[k] = (acc[k] * factor).astype(jnp.bfloat16)
        for j in range(1, size):
            part_copy(k, j).start()
        pump(1)

    own_rows = pl.ds(pl.multiple_of(me * rank_rows, rank_rows), rank_rows)
    for k in range(3):
        projected = acc[k, own_rows, :] * factor
        for j in range(1, size):
            part_copy(k, j).wait_recv()
            projected = projected + got[k, j - 1].astype(jnp.float32)
        one = 0.9 * m1_ref[k] + 0.1 * projected
        two = 0.9 * m2_ref[k] + 0.1 * projected * projected
        n1_ref[k] = one
        n2_ref[k] = two
        rounded = (one / (jnp.sqrt(two) + 1e-08)).astype(jnp.bfloat16)
        mine[k] = rounded
        dirs[k, own_rows, :] = rounded
        for way in range(2):
            dir_hop(k, 1, way).start()
    pump(3)
    for step in range(2, steps + 1):
        for k in range(3):
            for way in range(2):
                dir_hop(k, step - 1, way).wait_recv()
                dir_hop(k, step, way).start()
        if step == 3:
            pump(3)
    pump(len(forwards))
    for k in range(3):
        for way in range(2):
            dir_hop(k, steps, way).wait_recv()

    dirs_put = pltpu.make_async_copy(dirs, dirs_out, put_sem.at[3])
    dirs_put.start()

    row = lax.broadcasted_iota(jnp.int32, scale_ref.shape, 0)
    tile_sum = jnp.zeros(scale_ref.shape, jnp.float32)
    for k in range(3):
        values = dirs[k].astype(jnp.float32)
        tile_sum = tile_sum + jnp.where(row == k, jnp.sum(values * values), 0.0)
    sums[0] = tile_sum

    def sum_copy(j):
        return pltpu.make_async_remote_copy(
            src_ref=sums.at[0],
            dst_ref=sums.at[j],
            send_sem=sum_send.at[j],
            recv_sem=sum_recv.at[j],
            device_id=(me, lax.rem(mt + j, groups)),
            device_id_type=MESH,
        )

    for j in range(1, groups):
        sum_copy(j).start()
    total = tile_sum
    for j in range(1, groups):
        sum_copy(j).wait_recv()
        total = total + sums[j]
    scale_ref[...] = lax.rsqrt(total / entries + 1.0)

    for item in range(3):
        for way in range(2):
            weight_hop(item, steps, way).wait_recv()
    for put in puts:
        put.wait()
    dirs_put.wait()
    for k in range(3):
        for step in range(1, steps + 1):
            for way in range(2):
                weight_hop(k, step, way).wait_send()
                dir_hop(k, step, way).wait_send()
        for j in range(1, size):
            part_copy(k, j).wait_send()
    for j in range(1, groups):
        sum_copy(j).wait_send()


def exchange(size, groups, x, oc, fc, vc, go, bases, fw, vw, ow, m1, m2):
    tokens, width = x.shape
    rank = bases.shape[2]
    rows, columns = fw.shape
    rank_rows = m1.shape[1]
    steps = size // 2
    tiles = 4
    bf16, f32 = jnp.bfloat16, jnp.float32
    hbm = pl.BlockSpec(memory_space=pl.ANY)
    vmem = pl.BlockSpec(memory_space=pltpu.VMEM)
    dma = pltpu.SemaphoreType.DMA
    kernel = functools.partial(
        exchange_kernel,
        size,
        groups,
        float(tokens * size) ** (-0.5),
        float(rank * columns * groups),
    )
    return pl.pallas_call(
        kernel,
        out_shape=(
            jax.ShapeDtypeStruct((rows * size, columns), bf16),
            jax.ShapeDtypeStruct((rows * size, columns), bf16),
            jax.ShapeDtypeStruct((ow.shape[0], ow.shape[1] * size), bf16),
            jax.ShapeDtypeStruct((3, rank, columns), bf16),
            jax.ShapeDtypeStruct((8, 128), f32),
            jax.ShapeDtypeStruct(m1.shape, f32),
            jax.ShapeDtypeStruct(m2.shape, f32),
        ),
        in_specs=[hbm] * 6 + [vmem] * 5,
        out_specs=(hbm,) * 4 + (vmem,) * 3,
        scratch_shapes=[
            pltpu.VMEM(x.shape, bf16),
            pltpu.VMEM(oc.shape, bf16),
            pltpu.VMEM((3, tokens, columns), bf16),
            pltpu.VMEM(bases.shape, bf16),
            pltpu.VMEM(fw.shape, bf16),
            pltpu.VMEM(vw.shape, bf16),
            pltpu.VMEM(ow.shape, bf16),
            pltpu.VMEM((3, rank, columns), f32),
            pltpu.VMEM((3, rank, columns), bf16),
            pltpu.VMEM((3, size - 1, rank_rows, columns), bf16),
            pltpu.VMEM((3, rank_rows, columns), bf16),
            pltpu.VMEM((3, rank, columns), bf16),
            pltpu.VMEM((groups, 8, 128), f32),
            dma((5, tiles)),
            dma((3,)),
            dma((4,)),
            dma((2, 3, steps)),
            dma((2, 3, steps)),
            dma((3, size - 1)),
            dma((3, size - 1)),
            dma((2, 3, steps)),
            dma((2, 3, steps)),
            dma((groups,)),
            dma((groups,)),
        ],
        compiler_params=pltpu.CompilerParams(
            collective_id=0, has_side_effects=True, vmem_limit_bytes=46 * 1024 * 1024
        ),
    )(x, oc, fc, vc, go, bases, fw, vw, ow, m1, m2)


def on_device(
    normed_input,
    forget_cot,
    value_cot,
    gated_output,
    output_cot,
    forget_weight,
    value_weight,
    out_weight,
    bases,
    first_moment,
    second_moment,
):
    size, groups = lax.axis_size("fs"), lax.axis_size("tp")
    rows = forget_weight.shape[0]
    old_f, old_v, old_o, dirs, scales, one, two = exchange(
        size,
        groups,
        normed_input,
        output_cot,
        forget_cot,
        value_cot,
        gated_output,
        bases,
        forget_weight,
        value_weight,
        out_weight,
        first_moment.transpose(1, 0, 2),
        second_moment.transpose(1, 0, 2),
    )
    mine = lax.dynamic_slice_in_dim(bases, lax.axis_index("fs") * rows, rows, 1)
    f32 = jnp.float32

    def down(base, k):
        return jnp.dot(base[k], dirs[k], preferred_element_type=f32) * scales[k, 0]

    def across(base, k):
        return (
            lax.dot_general(dirs[k], base[k], (((0,), (1,)), ((), ())), preferred_element_type=f32)
            * scales[k, 0]
        )

    step_forget, step_value, step_out = down(mine, 0), down(mine, 1), across(mine, 2)
    return (
        forget_weight - 0.01 * step_forget,
        value_weight - 0.01 * step_value,
        out_weight - 0.01 * step_out,
        (old_f.astype(f32) - 0.01 * down(bases, 0)).astype(jnp.bfloat16),
        (old_v.astype(f32) - 0.01 * down(bases, 1)).astype(jnp.bfloat16),
        (old_o.astype(f32) - 0.01 * across(bases, 2)).astype(jnp.bfloat16),
        one.transpose(1, 0, 2),
        two.transpose(1, 0, 2),
        step_forget,
        step_value,
        step_out,
    )


def solution(mesh):
    placed = (
        P("fs", None),
        P("fs", "tp"),
        P("fs", "tp"),
        P("fs", "tp"),
        P("fs", None),
        P("fs", "tp"),
        P("fs", "tp"),
        P("tp", "fs"),
        P(),
        P("fs", None, "tp"),
        P("fs", None, "tp"),
    )
    return jax.shard_map(
        on_device,
        mesh=mesh,
        in_specs=placed,
        out_specs=(
            P("fs", "tp"),
            P("fs", "tp"),
            P("tp", "fs"),
            P(None, "tp"),
            P(None, "tp"),
            P("tp", None),
            P("fs", None, "tp"),
            P("fs", None, "tp"),
            P("fs", "tp"),
            P("fs", "tp"),
            P("tp", "fs"),
        ),
        check_vma=False,
    )
```

time: 340 us -> 137 us (0.40)
  waiting for transfers between devices: 219 us -> 0 us
  Pallas kernels: 0 us -> 95.3 us
  blocking collectives: 40.3 us -> 0 us
  local copies, waits for them, and re-layouts: 36.9 us -> 19.7 us
  between operations: 14.7 us -> 0.7 us
  other arithmetic: 6.41 us -> 0 us
    all_gather x4 -> x0, waiting for transfers between devices: 139 us -> none  [the longest x1 47.1 us: on_device(): lax.all_gather(new_value.astype(jnp.bfloat16), 'fs', axis=0, tiled=True)]
    pallas_call x0 -> x1, Pallas kernels: none -> 95.3 us  [exchange(): pl.pallas_call(kernel, out_shape=(jax.ShapeDtypeStruct((rows * size, colu...]
    unnamed x6 -> x0, waiting for transfers between devices: 80.4 us -> none
    psum x1 -> x0, blocking collectives: 40.3 us -> none  [on_device(): totals = lax.psum(jnp.sum(direction * direction, axis=(0, 2)), ('fs', 'tp'))]
    unnamed x54 -> x16, local copies, waits for them, and re-layouts: 34.2 us -> 12.7 us
    pallas_call x0 -> x2, local copies, waits for them, and re-layouts: none -> 6.27 us  [exchange(): pl.pallas_call(kernel, out_shape=(jax.ShapeDtypeStruct((rows * size, colu...]
    convert_element_type x4 -> x0, other arithmetic: 5.47 us -> none  [the longest x2 2.28 us: split_parts(): high = lax.optimization_barrier(values.astype(jnp.bfloat16))]
    dot_general x7 -> x6, matrix products: 21.8 us -> 21.2 us  [the longest x4 13.7 us: down(): return jnp.dot(base[k], dirs[k], preferred_element_type=f32) * scales[k, 0]]
  transfers between devices with their start and end apart: 5 -> 0, of which waited for: 5 -> 0; matrix products, arithmetic and copies ran while one was open for 5% -> 0% of each run, Pallas kernels for 0% -> 0%
where the time goes in v1:
time: 137 us
  Pallas kernels  95.3 us (70%)
  matrix products  21.2 us (15%)
  local copies, waits for them, and re-layouts  19.7 us (14%)
    pallas_call x1, Pallas kernels, exchange(): pl.pallas_call(kernel, out_shape=(jax.ShapeDtypeStruct((rows * size, colu...  95.3 us
    dot_general x4, matrix products, down(): return jnp.dot(base[k], dirs[k], preferred_element_type=f32) * scales[k, 0]  13.7 us
    unnamed x16, local copies, waits for them, and re-layouts  12.7 us
    dot_general x2, matrix products, across(): lax.dot_general(dirs[k], base[k], (((0,), (1,)), ((), ())), preferred_ele...  7.56 us
    pallas_call x2, local copies, waits for them, and re-layouts, exchange(): pl.pallas_call(kernel, out_shape=(jax.ShapeDtypeStruct((rows * size, colu...  6.27 us

profile of v1, /device:TPU:0, one launch (start us, length us, event | category | flops | bytes accessed | tf_op | source)
XLA Modules:
  0.0 136.9 jit_solution(6971429786469580970)
XLA Ops:
  0.7 0.0 copy-start
  0.7 1.0 copy-done
  1.7 0.0 copy-start.1
  1.7 1.0 copy-done.1
  2.7 0.0 copy-start.2
  2.7 1.0 copy-done.2
  3.8 0.0 copy-start.4
  3.8 0.9 copy-done.4
  4.7 0.0 copy-start.5
  4.7 0.9 copy-done.5
  5.6 95.3 %shard_map.194 = (bf16[2048,512]{1,0:T(8,128)(2,1)S(1)}, bf16[2048,512]{1,0:T(8,128)(2,1)S(1)}, bf16[512,2048]{1,0:T(8,128)(2,1)}, bf16[3,256,512]{2,1,0:T(8,128...) custom-call(bf16[2048,2048]{1,0:T(8,128)(2,1)} %x_hbm.1, ...), custom_call_target="tpu_custom_call" | custom-call | tf_op jit(solution)/shard_map/pallas_call | solution.py:326
  100.9 0.0 copy-start.3
  100.9 0.7 fusion.23
  101.6 4.8 %subtract_convert_fusion = bf16[512,2048]{1,0:T(8,128)(2,1)} fusion(bf16[512,2048]{1,0:T(8,128)(2,1)} %get-tuple-element.22, f32[]{:T(128)} %bitcast.10, bf16[3,2048,256]{2,1,0:T(8,128)(2,1)} %bases_hbm.1, bf16[3,256,512]{2,1,0:T(8,128)(2,1)S(1)} %get-tuple-element.18), kind=kOutput, calls=%fused_computation.4 | convolution fusion | flops 542113792 | bytes 5505536 | tf_op jit(solution)/shard_map/dot_general | solution.py:409
  106.4 0.0 copy-done.3
  106.4 2.8 %multiply_subtract_fusion = (f32[512,256]{1,0:T(8,128)}, f32[512,256]{1,0:T(8,128)}) fusion(f32[512,256]{1,0:T(8,128)S(1)} %copy-done.1, f32[]{:T(128)} %bitcast.10, bf16[3,2048,256]{2,1,0:T(8,128)(2,1)} %bases_hbm.1, s32[]{:T(128)S(6)} %add.5, s32[]{:T(128)S(6)} %select_n.3, bf16[3,256,512]{2,1,0:T(8,128)(2,1)S(1)} %get-tuple-element.18), kind=kOutput, calls=%fused_computation.14 | convolution fusion | flops 67502080 | bytes 1966600 | tf_op jit(solution)/shard_map/dot_general | solution.py:409
  109.1 2.7 %multiply_subtract_fusion.1 = (f32[256,512]{1,0:T(8,128)}, f32[256,512]{1,0:T(8,128)}) fusion(f32[256,512]{1,0:T(8,128)S(1)} %copy-done.2, f32[]{:T(128)} %bitcast.7, bf16[3,256,512]{2,1,0:T(8,128)(2,1)S(1)} %get-tuple-element.18, bf16[3,2048,256]{2,1,0:T(8,128)(2,1)} %bases_hbm.1, s32[]{:T(128)S(6)} %add.4, s32[]{:T(128)S(6)} %select_n.3), kind=kOutput, calls=%fused_computation.15 | convolution fusion | flops 67502080 | bytes 1966600 | tf_op jit(solution)/shard_map/dot_general | solution.py:405
  111.9 2.8 %multiply_subtract_fusion.2 = (f32[256,512]{1,0:T(8,128)}, f32[256,512]{1,0:T(8,128)}) fusion(f32[256,512]{1,0:T(8,128)S(1)} %copy-done, f32[]{:T(128)} %bitcast.4, bf16[3,256,512]{2,1,0:T(8,128)(2,1)S(1)} %get-tuple-element.18, bf16[3,2048,256]{2,1,0:T(8,128)(2,1)} %bases_hbm.1, s32[]{:T(128)S(6)} %select_n.3), kind=kOutput, calls=%fused_computation.16 | convolution fusion | flops 67502080 | bytes 1966596 | tf_op jit(solution)/shard_map/dot_general | solution.py:405
  114.7 3.9 %copy.22 = bf16[2048,512]{0,1:T(8,128)(2,1)} copy(bf16[2048,512]{1,0:T(8,128)(2,1)} %copy-done.3) | data formatting | bytes 4194304 | tf_op jit(solution)/shard_map/pallas_call | solution.py:326
  118.6 4.8 %fusion.1 = bf16[2048,512]{0,1:T(8,128)(2,1)} fusion(bf16[2048,512]{0,1:T(8,128)(2,1)} %copy.22, f32[]{:T(128)} %bitcast.4, bf16[3,2048,256]{2,1,0:T(8,128)(2,1)} %bases_hbm.1, bf16[3,256,512]{2,1,0:T(8,128)(2,1)S(1)} %get-tuple-element.18), kind=kOutput, calls=%fused_computation.3 | convolution fusion | flops 542113792 | bytes 5505536 | tf_op jit(solution)/shard_map/dot_general | solution.py:405
  123.3 3.9 %copy.24 = bf16[2048,512]{1,0:T(8,128)(2,1)} copy(bf16[2048,512]{0,1:T(8,128)(2,1)} %fusion.1) | data formatting | bytes 4194304
  127.2 2.4 %copy.23 = bf16[2048,512]{0,1:T(8,128)(2,1)} copy(bf16[2048,512]{1,0:T(8,128)(2,1)S(1)} %get-tuple-element.21) | data formatting | bytes 4194304 | tf_op jit(solution)/shard_map/pallas_call | solution.py:326
  129.6 3.4 %fusion = bf16[2048,512]{0,1:T(8,128)(2,1)S(1)} fusion(bf16[2048,512]{0,1:T(8,128)(2,1)} %copy.23, f32[]{:T(128)} %bitcast.7, bf16[3,2048,256]{2,1,0:T(8,128)(2,1)} %bases_hbm.1, bf16[3,256,512]{2,1,0:T(8,128)(2,1)S(1)} %get-tuple-element.18), kind=kOutput, calls=%fused_computation.1 | convolution fusion | flops 542113792 | bytes 5505536 | tf_op jit(solution)/shard_map/dot_general | solution.py:405
  133.0 2.5 %copy.25 = bf16[2048,512]{1,0:T(8,128)(2,1)} copy(bf16[2048,512]{0,1:T(8,128)(2,1)S(1)} %fusion) | data formatting | bytes 4194304
  135.5 0.7 copy.28
  136.2 0.7 copy.29
Async XLA Ops:
  0.7 1.0 copy-start
  1.7 1.0 copy-start.1
  2.7 1.0 copy-start.2
  3.8 0.9 copy-start.4
  4.7 0.9 copy-start.5
  100.9 5.4 %copy-start.3 = (bf16[2048,512]{1,0:T(8,128)(2,1)}, bf16[2048,512]{1,0:T(8,128)(2,1)S(1)}, u32[]{:S(2)}) copy-start(bf16[2048,512]{1,0:T(8,128)(2,1)S(1)} %get-tuple-element.20) | copy-start | bytes 6291460

commit v2 on v1

--- a/solution.py
+++ b/solution.py
@@ -32,11 +32,11 @@
     vc_hbm,
     go_hbm,
     bases_hbm,
-    fw_ref,
-    vw_ref,
-    ow_ref,
-    m1_ref,
-    m2_ref,
+    fw_hbm,
+    vw_hbm,
+    ow_hbm,
+    m1_hbm,
+    m2_hbm,
     all_f,
     all_v,
     all_o,
@@ -44,6 +44,12 @@
     scale_ref,
     n1_ref,
     n2_ref,
+    fw_ref,
+    vw_ref,
+    ow_ref,
+    m1_ref,
+    m2_ref,
+    first_sem,
     x_buf,
     oc_buf,
     c_buf,
@@ -81,7 +87,20 @@
     rank_rows = m1_ref.shape[1]
     columns = m1_ref.shape[2]
 
-    loads = []
+    firsts = [
+        pltpu.make_async_copy(src, dst, first_sem.at[i])
+        for i, (src, dst) in enumerate(
+            (
+                (fw_hbm, fw_ref),
+                (vw_hbm, vw_ref),
+                (ow_hbm, ow_ref),
+                (m1_hbm, m1_ref),
+                (m2_hbm, m2_ref),
+            )
+        )
+    ]
+    for copy in firsts[:3]:
+        copy.start()
     base_copies = [
         pltpu.make_async_copy(bases_hbm.at[k], b_buf.at[k], base_sem.at[k]) for k in range(3)
     ]
@@ -109,6 +128,9 @@
         for which in (3, 4):
             load(which, *streams[which], tile).start()
 
+    for copy in firsts[3:]:
+        copy.start()
+
     barrier = pltpu.get_barrier_semaphore()
     for j in range(1, size):
         pl.semaphore_signal(
@@ -118,6 +140,8 @@
         pl.semaphore_signal(
             barrier, inc=1, device_id=(me, lax.rem(mt + j, groups)), device_id_type=MESH
         )
+    for copy in firsts[:3]:
+        copy.wait()
     wf_buf[...] = fw_ref[...].astype(jnp.bfloat16)
     wv_buf[...] = vw_ref[...].astype(jnp.bfloat16)
     wo_buf[...] = ow_ref[...].astype(jnp.bfloat16)
@@ -203,6 +227,23 @@
             device_id=(owner, mt),
             device_id_type=MESH,
         )
+
+    own_rows = pl.ds(pl.multiple_of(me * rank_rows, rank_rows), rank_rows)
+
+    def combine(k):
+        projected = acc[k, own_rows, :] * factor
+        for j in range(1, size):
+            part_copy(k, j).wait_recv()
+            projected = projected + got[k, j - 1].astype(jnp.float32)
+        one = 0.9 * m1_ref[k] + 0.1 * projected
+        two = 0.9 * m2_ref[k] + 0.1 * projected * projected
+        n1_ref[k] = one
+        n2_ref[k] = two
+        rounded = (one / (jnp.sqrt(two) + 1e-08)).astype(jnp.bfloat16)
+        mine[k] = rounded
+        dirs[k, own_rows, :] = rounded
+        for way in range(2):
+            dir_hop(k, 1, way).start()
 
     for k in range(3):
         base_copies[k].wait()
@@ -231,23 +272,15 @@
         for j in range(1, size):
             part_copy(k, j).start()
         pump(1)
-
-    own_rows = pl.ds(pl.multiple_of(me * rank_rows, rank_rows), rank_rows)
-    for k in range(3):
-        projected = acc[k, own_rows, :] * factor
-        for j in range(1, size):
-            part_copy(k, j).wait_recv()
-            projected = projected + got[k, j - 1].astype(jnp.float32)
-        one = 0.9 * m1_ref[k] + 0.1 * projected
-        two = 0.9 * m2_ref[k] + 0.1 * projected * projected
-        n1_ref[k] = one
-        n2_ref[k] = two
-        rounded = (one / (jnp.sqrt(two) + 1e-08)).astype(jnp.bfloat16)
-        mine[k] = rounded
-        dirs[k, own_rows, :] = rounded
-        for way in range(2):
-            dir_hop(k, 1, way).start()
-    pump(3)
+        if k == 1:
+            for copy in firsts[3:]:
+                copy.wait()
+        if k > 0:
+            combine(k - 1)
+
+    pump(1)
+    combine(2)
+    pump(2)
     for step in range(2, steps + 1):
         for k in range(3):
             for way in range(2):
@@ -334,9 +367,15 @@
             jax.ShapeDtypeStruct(m1.shape, f32),
             jax.ShapeDtypeStruct(m2.shape, f32),
         ),
-        in_specs=[hbm] * 6 + [vmem] * 5,
+        in_specs=[pl.BlockSpec(memory_space=pltpu.HBM)] * 11,
         out_specs=(hbm,) * 4 + (vmem,) * 3,
         scratch_shapes=[
+            pltpu.VMEM(fw.shape, f32),
+            pltpu.VMEM(vw.shape, f32),
+            pltpu.VMEM(ow.shape, f32),
+            pltpu.VMEM(m1.shape, f32),
+            pltpu.VMEM(m2.shape, f32),
+            dma((5,)),
             pltpu.VMEM(x.shape, bf16),
             pltpu.VMEM(oc.shape, bf16),
             pltpu.VMEM((3, tokens, columns), bf16),
@@ -363,9 +402,186 @@
             dma((groups,)),
         ],
         compiler_params=pltpu.CompilerParams(
-            collective_id=0, has_side_effects=True, vmem_limit_bytes=46 * 1024 * 1024
+            collective_id=0, has_side_effects=True, vmem_limit_bytes=54 * 1024 * 1024
         ),
     )(x, oc, fc, vc, go, bases, fw, vw, ow, m1, m2)
+
+
+def finish_kernel(
+    scale_hbm,
+    dirs_hbm,
+    f_hbm,
+    v_hbm,
+    o_hbm,
+    n1_hbm,
+    n2_hbm,
+    bases_hbm,
+    fw_hbm,
+    vw_hbm,
+    ow_hbm,
+    new_f,
+    new_v,
+    new_o,
+    copy_f,
+    copy_v,
+    copy_o,
+    n1_out,
+    n2_out,
+    step_f,
+    step_v,
+    step_o,
+    scale_ref,
+    dirs_ref,
+    bases_ref,
+    fw_ref,
+    vw_ref,
+    ow_ref,
+    f_ref,
+    v_ref,
+    o_ref,
+    n1_ref,
+    n2_ref,
+    small_sem,
+    load_sem,
+    cf_buf,
+    cv_buf,
+    co_buf,
+    down_buf,
+    across_buf,
+    tile_sem,
+    own_sem,
+):
+    tiles = tile_sem.shape[1]
+    rows = f_ref.shape[0] // tiles
+    smalls = [
+        pltpu.make_async_copy(src, dst, small_sem.at[i])
+        for i, (src, dst) in enumerate(
+            (
+                (dirs_hbm, dirs_ref),
+                (scale_hbm, scale_ref),
+                (bases_hbm, bases_ref),
+                (fw_hbm, fw_ref),
+                (vw_hbm, vw_ref),
+                (ow_hbm, ow_ref),
+                (n1_hbm, n1_ref),
+                (n2_hbm, n2_ref),
+            )
+        )
+    ]
+    loads = []
+    for tile in range(tiles):
+        at = pl.ds(tile * rows, rows)
+        views = (
+            (f_hbm.at[at, :], f_ref.at[at, :]),
+            (v_hbm.at[at, :], v_ref.at[at, :]),
+            (o_hbm.at[:, at], o_ref.at[:, at]),
+        )
+        loads.append(
+            [
+                pltpu.make_async_copy(src, dst, load_sem.at[i, tile])
+                for i, (src, dst) in enumerate(views)
+            ]
+        )
+    for copy in smalls:
+        copy.start()
+    for group in loads:
+        for copy in group:
+            copy.start()
+    for copy in smalls[:6]:
+        copy.wait()
+    copies = []
+
+    def put(src, dst, sem):
+        copy = pltpu.make_async_copy(src, dst, sem)
+        copy.start()
+        copies.append(copy)
+
+    def down(rows, k):
+        step = jnp.dot(bases_ref[k, rows, :], dirs_ref[k], preferred_element_type=jnp.float32)
+        return step * scale_ref[k : k + 1, 0:1]
+
+    def across(rows):
+        step = lax.dot_general(
+            dirs_ref[2],
+            bases_ref[2, rows, :],
+            (((0,), (1,)), ((), ())),
+            preferred_element_type=jnp.float32,
+        )
+        return step * scale_ref[2:3, 0:1]
+
+    own = fw_ref.shape[0]
+    me = pl.ds(pl.multiple_of(lax.axis_index("fs") * own, own), own)
+    for k, weight, new, out in ((0, fw_ref, new_f, step_f), (1, vw_ref, new_v, step_v)):
+        step = down(me, k)
+        down_buf[2 * k] = step
+        put(down_buf.at[2 * k], out, own_sem.at[2 * k])
+        down_buf[2 * k + 1] = weight[...] - 0.01 * step
+        put(down_buf.at[2 * k + 1], new, own_sem.at[2 * k + 1])
+    step = across(me)
+    across_buf[0] = step
+    put(across_buf.at[0], step_o, own_sem.at[4])
+    across_buf[1] = ow_ref[...] - 0.01 * step
+    put(across_buf.at[1], new_o, own_sem.at[5])
+
+    for copy in smalls[6:]:
+        copy.wait()
+    put(n1_ref, n1_out, own_sem.at[6])
+    put(n2_ref, n2_out, own_sem.at[7])
+
+    for tile in range(tiles):
+        at = pl.ds(tile * rows, rows)
+        for copy in loads[tile]:
+            copy.wait()
+        for k, old, buf, out in ((0, f_ref, cf_buf, copy_f), (1, v_ref, cv_buf, copy_v)):
+            value = old[at, :].astype(jnp.float32) - 0.01 * down(at, k)
+            buf[at, :] = value.astype(jnp.bfloat16)
+            put(buf.at[at, :], out.at[at, :], tile_sem.at[k, tile])
+        value = o_ref[:, at].astype(jnp.float32) - 0.01 * across(at)
+        co_buf[:, at] = value.astype(jnp.bfloat16)
+        put(co_buf.at[:, at], copy_o.at[:, at], tile_sem.at[2, tile])
+    for copy in copies:
+        copy.wait()
+
+
+def finish(scales, dirs, bases, old_f, old_v, old_o, fw, vw, ow, one, two):
+    tiles = 4
+    depth, columns = old_f.shape
+    rank = bases.shape[2]
+    dma = pltpu.SemaphoreType.DMA
+    hbm = pl.BlockSpec(memory_space=pltpu.HBM)
+    outs = (fw, vw, ow, old_f, old_v, old_o, one, two, fw, vw, ow)
+    return pl.pallas_call(
+        finish_kernel,
+        out_shape=tuple(jax.ShapeDtypeStruct(a.shape, a.dtype) for a in outs),
+        in_specs=[hbm] * 11,
+        out_specs=(pl.BlockSpec(memory_space=pltpu.HBM),) * 11,
+        scratch_shapes=[
+            pltpu.VMEM(scales.shape, jnp.float32),
+            pltpu.VMEM(dirs.shape, jnp.bfloat16),
+            pltpu.VMEM(bases.shape, jnp.bfloat16),
+            pltpu.VMEM(fw.shape, jnp.float32),
+            pltpu.VMEM(vw.shape, jnp.float32),
+            pltpu.VMEM(ow.shape, jnp.float32),
+            pltpu.VMEM(old_f.shape, jnp.bfloat16),
+            pltpu.VMEM(old_v.shape, jnp.bfloat16),
+            pltpu.VMEM(old_o.shape, jnp.bfloat16),
+            pltpu.VMEM(one.shape, jnp.float32),
+            pltpu.VMEM(two.shape, jnp.float32),
+            dma((8,)),
+            dma((3, tiles)),
+            pltpu.VMEM(old_f.shape, jnp.bfloat16),
+            pltpu.VMEM(old_v.shape, jnp.bfloat16),
+            pltpu.VMEM(old_o.shape, jnp.bfloat16),
+            pltpu.VMEM((4,) + fw.shape, jnp.float32),
+            pltpu.VMEM((2,) + ow.shape, jnp.float32),
+            dma((3, tiles)),
+            dma((8,)),
+        ],
+        compiler_params=pltpu.CompilerParams(vmem_limit_bytes=56 * 1024 * 1024),
+        cost_estimate=pl.CostEstimate(
+            flops=6 * depth * rank * columns, bytes_accessed=16 * depth * columns, transcendentals=0
+        ),
+    )(scales, dirs, old_f, old_v, old_o, one, two, bases, fw, vw, ow)
 
 
 def on_device(
@@ -382,7 +598,6 @@
     second_moment,
 ):
     size, groups = lax.axis_size("fs"), lax.axis_size("tp")
-    rows = forget_weight.shape[0]
     old_f, old_v, old_o, dirs, scales, one, two = exchange(
         size,
         groups,
@@ -398,31 +613,24 @@
         first_moment.transpose(1, 0, 2),
         second_moment.transpose(1, 0, 2),
     )
-    mine = lax.dynamic_slice_in_dim(bases, lax.axis_index("fs") * rows, rows, 1)
-    f32 = jnp.float32
-
-    def down(base, k):
-        return jnp.dot(base[k], dirs[k], preferred_element_type=f32) * scales[k, 0]
-
-    def across(base, k):
-        return (
-            lax.dot_general(dirs[k], base[k], (((0,), (1,)), ((), ())), preferred_element_type=f32)
-            * scales[k, 0]
-        )
-
-    step_forget, step_value, step_out = down(mine, 0), down(mine, 1), across(mine, 2)
+    outs = finish(
+        scales,
+        dirs,
+        bases,
+        old_f,
+        old_v,
+        old_o,
+        forget_weight,
+        value_weight,
+        out_weight,
+        one,
+        two,
+    )
     return (
-        forget_weight - 0.01 * step_forget,
-        value_weight - 0.01 * step_value,
-        out_weight - 0.01 * step_out,
-        (old_f.astype(f32) - 0.01 * down(bases, 0)).astype(jnp.bfloat16),
-        (old_v.astype(f32) - 0.01 * down(bases, 1)).astype(jnp.bfloat16),
-        (old_o.astype(f32) - 0.01 * across(bases, 2)).astype(jnp.bfloat16),
-        one.transpose(1, 0, 2),
-        two.transpose(1, 0, 2),
-        step_forget,
-        step_value,
-        step_out,
+        *outs[:6],
+        outs[6].transpose(1, 0, 2),
+        outs[7].transpose(1, 0, 2),
+        *outs[8:],
     )
 
 

time: 137 us -> 110 us (0.80)
  matrix products: 21.2 us -> 0 us
  local copies, waits for them, and re-layouts: 19.7 us -> 0 us
  Pallas kernels: 95.3 us -> 109 us
    dot_general x6 -> x0, matrix products: 21.2 us -> none  [the longest x4 13.7 us: down(): return jnp.dot(base[k], dirs[k], preferred_element_type=f32) * scales[k, 0]]
    unnamed x16 -> x0, local copies, waits for them, and re-layouts: 12.7 us -> none
    pallas_call x0 -> x1, Pallas kernels: none -> 8.31 us  [finish(): pl.pallas_call(finish_kernel, out_shape=tuple((jax.ShapeDtypeStruct(a.sha...]
    pallas_call x2 -> x0, local copies, waits for them, and re-layouts: 6.27 us -> none  [exchange(): pl.pallas_call(kernel, out_shape=(jax.ShapeDtypeStruct((rows * size, colu...]
    pallas_call x1, Pallas kernels: 95.3 us -> 101 us  [exchange(): pl.pallas_call(kernel, out_shape=(jax.ShapeDtypeStruct((rows * size, colu...]
where the time goes in v2:
time: 110 us
  Pallas kernels  109 us (99%)
    pallas_call x1, Pallas kernels, exchange(): pl.pallas_call(kernel, out_shape=(jax.ShapeDtypeStruct((rows * size, colu...  101 us
    pallas_call x1, Pallas kernels, finish(): pl.pallas_call(finish_kernel, out_shape=tuple((jax.ShapeDtypeStruct(a.sha...  8.31 us

profile of v2, /device:TPU:0, one launch (start us, length us, event | category | flops | bytes accessed | tf_op | source)
XLA Modules:
  0.0 110.1 jit_solution(17852121015792840984)
XLA Ops:
  0.6 101.2 %shard_map.194 = (bf16[2048,512]{1,0:T(8,128)(2,1)}, bf16[2048,512]{1,0:T(8,128)(2,1)}, bf16[512,2048]{1,0:T(8,128)(2,1)}, bf16[3,256,512]{2,1,0:T(8,128)(2,1)},...) custom-call(bf16[2048,2048]{1,0:T(8,128)(2,1)} %x_hbm.1, bf16[2048,2048]{1,0:T(8,128)(2,1)} %oc_hbm.1, ...), custom_call_target="tpu_custom_call" | custom-call | tf_op jit(solution)/shard_map/pallas_call | solution.py:359
  101.8 8.3 %shard_map.195 = (f32[256,512]{1,0:T(8,128)}, f32[256,512]{1,0:T(8,128)}, f32[512,256]{1,0:T(8,128)}, bf16[2048,512]{1,0:T(8,128)(2,1)}, bf16[2048,512]{1,0:T(8,...) custom-call(f32[8,128]{1,0:T(8,128)} %get-tuple-element.29.scale_hbm, ...), custom_call_target="tpu_custom_call" | custom-call | flops 1610612736 | bytes 16777216 | tf_op jit(solution)/shard_map/pallas_call | solution.py:553
